TPU v7x, 32 devices: a whole 2x2x4 slice. The times are simulated.
32 devices in a mesh: fs: 4 (over y, x), tp: 8 (over z, core).
Axes of the slice: x: 2, y: 2, z: 4, core: 2. Of those that a mesh axis runs over, the one named last changes fastest.
Arguments:
- inputs: bfloat16 [1536, 2048], P('fs'), may hold values from -6 to 6
- pre_act: bfloat16 [1536, 8192], P('fs', 'tp'), may hold values from -6 to 6
- cotangent: bfloat16 [1536, 2048], P('fs'), may hold values from -6 to 6
- up_weight: bfloat16 [2048, 8192], P('fs', 'tp'), may hold values from -0.125 to 0.125
- down_weight: bfloat16 [8192, 2048], P('tp', 'fs'), may hold values from -0.0625 to 0.0625
Outputs:
- input_grad: bfloat16 [1536, 2048], P('fs')
- up_grad: float32 [2048, 8192], P('fs', 'tp')
- down_grad: float32 [8192, 2048], P('tp', 'fs')
- up_norms: float32 [2048], P('fs')
- down_norms: float32 [8192], P('tp')
All inputs are finite; a program needn't handle non-finite values.
Results may differ from a plain program's by a relative error of at most 0.0051.
Values may be sent and summed in bfloat16 or wider, within the bound.
A program may use at most 64 MiB of HBM per device.

v0:
```python
import functools

import jax
import jax.numpy as jnp
from jax import lax
from jax.experimental import pallas as pl
from jax.experimental.pallas import tpu as pltpu
from jax.sharding import PartitionSpec as P

MESH = pl.DeviceIdType.MESH
F32, BF16 = jnp.float32, jnp.bfloat16


def contract_last(left, right):
    return lax.dot_general(left, right, (((1,), (1,)), ((), ())), preferred_element_type=F32)


def contract_first(left, right):
    return lax.dot_general(left, right, (((0,), (0,)), ((), ())), preferred_element_type=F32)


def bits_of(n):
    return [1 << i for i in range(n.bit_length() - 1)]


def by_weight(n, down=False):
    return sorted(range(1, n), key=lambda m: (bin(m).count("1"), -m if down else m))


class Gather:
    def __init__(self, n, me, device, source, place, send, recv, orders):
        self.n, self.me, self.device = n, me, device
        self.source, self.place = source, place
        self.send, self.recv, self.orders = send, recv, orders
        self.started = []

    def targets(self, cls, m):
        bits = bits_of(self.n)
        if m == 0:
            return bits
        if self.orders[cls] == "up":
            return [b for b in bits if b > m]
        return [b for b in bits if b < (m & -m)]

    def copy(self, cls, m, b):
        there = self.place(self.me ^ m, cls)
        return pltpu.make_async_remote_copy(
            src_ref=self.source(cls) if m == 0 else there,
            dst_ref=there,
            send_sem=self.send(cls, m ^ b),
            recv_sem=self.recv(cls, m ^ b),
            device_id=self.device(self.me ^ b),
            device_id_type=MESH,
        )

    def push(self, cls, m, only=None):
        for b in self.targets(cls, m):
            if only is None or b == only:
                copy = self.copy(cls, m, b)
                copy.start()
                self.started.append(copy)

    def push_own(self, turns=None):
        classes = list(range(len(self.orders)))
        for i, b in enumerate(bits_of(self.n)):
            for j, cls in enumerate(classes if i % 2 == 0 else classes[::-1]):
                if turns is None or j in turns:
                    self.push(cls, 0, b)

    def arrive(self, cls, m):
        here = self.place(self.me ^ m, cls)
        pltpu.make_async_remote_copy(
            src_ref=here,
            dst_ref=here,
            send_sem=self.send(cls, m),
            recv_sem=self.recv(cls, m),
            device_id=self.device(self.me ^ (m & -m)),
            device_id_type=MESH,
        ).wait_recv()

    def drain(self):
        for copy in self.started:
            copy.wait_send()


def share_rows(rows, parts):
    cuts = 1
    while cuts < parts and rows % (2 * cuts * 16) == 0:
        cuts *= 2
    return cuts


def piece_shape(nt, rows, db):
    nz = nt // 2
    if db % (128 * nz) == 0:
        return rows // 2, db // nz
    return rows // nt, db


def fused_kernel(nf, nt, subs, strips, cot, dw, pa, inp, up, ugrad, dgrad, got, un_all, dn_all,
                 cot_all, dw_all, pa_all, inp_all, up_all, pre, sqr, sq,
                 part, from_sib, wire, landed, final, un_own, dn_own,
                 xs, xr, zs, zr, ss, sr, a_s, a_r, bs, br, hs, hr, ws, wr, ts, tr, gs, gr, ks, kr,
                 us, ur, ds, dr, local_sem):
    f, t = lax.axis_index("fs"), lax.axis_index("tp")
    z, c = t // 2, t % 2
    nz = nt // 2
    rows, d = cot.shape
    ff, db = dw.shape
    half = rows // subs
    pr, pc = part.shape[3:]
    own_cols = pl.ds(pl.multiple_of(f * db, db), db)

    def remote(src, dst, send, recv, device):
        return pltpu.make_async_remote_copy(src_ref=src, dst_ref=dst, send_sem=send, recv_sem=recv,
                                            device_id=device, device_id_type=MESH)

    def columns(g, side):
        ih = rows // 2
        return inp.at[pl.ds(pl.multiple_of(side * ih, ih), ih), pl.ds(pl.multiple_of(g * db, db), db)]

    def in_half(g, side):
        ih = rows // 2
        return inp_all.at[g, pl.ds(pl.multiple_of(side * ih, ih), ih), :]

    own = [
        pltpu.make_async_copy(dw, dw_all.at[:, own_cols], local_sem.at[0]),
        pltpu.make_async_copy(cot, cot_all.at[f], local_sem.at[1]),
        pltpu.make_async_copy(pa, pa_all.at[f], local_sem.at[2]),
        pltpu.make_async_copy(up, up_all, local_sem.at[3]),
        pltpu.make_async_copy(columns(f, 0), in_half(f, 0), local_sem.at[4]),
        pltpu.make_async_copy(columns(f, 1), in_half(f, 1), local_sem.at[5]),
    ]
    for copy in own:
        copy.start()

    barrier = pltpu.get_barrier_semaphore()
    peers = [(f ^ m, t) for m in range(1, nf)] + [(f, t ^ m) for m in range(1, nt)]
    for peer in peers:
        pl.semaphore_signal(barrier, inc=1, device_id=peer, device_id_type=MESH)
    pl.semaphore_wait(barrier, len(peers))

    row_cuts = share_rows(rows, nt)
    col_cuts = nt // row_cuts
    cr, cc = rows // row_cuts, d // col_cuts

    def piece(ref, y, h=None):
        row = pl.multiple_of((y // col_cuts) * cr, cr)
        width = cc if h is None else cc // 2
        col = (y % col_cuts) * cc + (0 if h is None else h * width)
        return ref.at[pl.ds(row, cr), pl.ds(pl.multiple_of(col, width), width)]

    dwh = ff // 2
    pah = rows // 2

    def over_fs(k, source, place):
        return Gather(nf, f, lambda g: (g, t), source, place,
                      lambda cls, m: xs.at[k, cls, m], lambda cls, m: xr.at[k, cls, m], ("up", "down"))

    g_cot = over_fs(0, lambda h: piece(cot, t, h), lambda g, h: piece(cot_all.at[g], t, h))
    g_dw = over_fs(1, lambda h: dw.at[pl.ds(h * dwh, dwh), :],
                   lambda g, h: dw_all.at[pl.ds(h * dwh, dwh), pl.ds(pl.multiple_of(g * db, db), db)])
    g_pa = over_fs(2, lambda h: pa.at[pl.ds(h * pah, pah), :],
                   lambda g, h: pa_all.at[g, pl.ds(h * pah, pah), :])

    def strip(m, s, y):
        return piece(cot_all.at[f ^ m], y, s if strips == 2 else None)

    def over_z(m, s):
        spot = lambda y, cls=0: strip(m, s, 2 * y + c)
        return Gather(nz, z, lambda y: (f, 2 * y + c), lambda cls: spot(z), spot,
                      lambda cls, k: zs.at[m, s, k], lambda cls, k: zr.at[m, s, k], ("down",))

    def to_sibling(m, s, k):
        spot = strip(m, s, 2 * (z ^ k) + c)
        return remote(spot, spot, ss.at[m, s, k], sr.at[m, s, k], (f, t ^ 1))

    def from_sibling(m, s, k):
        spot = strip(m, s, 2 * (z ^ k) + 1 - c)
        return remote(spot, spot, ss.at[m, s, k], sr.at[m, s, k], (f, t ^ 1))

    exchange = lambda m: remote(columns(f ^ m, c), in_half(f, c), a_s.at[m], a_r.at[m], (f ^ m, t))
    exchanged = lambda m: remote(in_half(f ^ m, c), in_half(f ^ m, c), a_s.at[m], a_r.at[m], (f ^ m, t))
    in_to = lambda m: remote(in_half(f ^ m, c), in_half(f ^ m, c), bs.at[m], br.at[m], (f, t ^ 1))
    in_from = lambda m: remote(in_half(f ^ m, 1 - c), in_half(f ^ m, 1 - c), bs.at[m], br.at[m], (f, t ^ 1))

    masks = by_weight(nf)
    zorder = by_weight(nz, True)
    left = {m: 2 for m in masks}
    rings = {(m, s): over_z(m, s) for m in masks for s in range(strips)}
    singles = [m for m in masks if m & (m - 1) == 0]
    pairs = [(m, cls) for m in masks for cls in (0, 1)]
    inner = [p for p in pairs if g_dw.targets(p[1], p[0])]
    outer = [p for p in pairs if p not in inner]

    def take_cot(items):
        for m, cls in items:
            g_cot.arrive(cls, m)
            g_cot.push(cls, m)
            left[m] -= 1
            if strips == 2:
                rings[m, cls].push(0, 0)
                to_sibling(m, cls, 0).start()
            elif left[m] == 0:
                rings[m, 0].push(0, 0)
                to_sibling(m, 0, 0).start()

    def turn(m, s, steps):
        for k in steps:
            rings[m, s].arrive(0, k)
            rings[m, s].push(0, k)
            to_sibling(m, s, k).start()

    def take(g, items):
        for m, cls in items:
            g.arrive(cls, m)
            g.push(cls, m)

    tile = min(ff, 256)

    def square_grad(m):
        g = f ^ m
        if m:
            for s in range(strips):
                for k in range(nz):
                    from_sibling(m, s, k).wait_recv()
        sq[g] = contract_last(cot_all[g], dw_all[...])

    def unit(u):
        m, h = u
        g = f ^ m
        i = m * subs + h
        some = pl.ds(h * half, half)
        for j in range(ff // tile):
            cols = pl.ds(j * tile, tile)
            active = jnp.maximum(pa_all[g, some, cols].astype(F32), 0.0)
            pre[g, some, cols] = (2.0 * active * sq[g, some, cols]).astype(BF16)
            sqr[g, some, cols] = (active * active).astype(BF16)
        total = contract_last(pre[g, some, :], up_all[...])
        wide = half // 2 == pr
        for k in range(nt):
            row, col = ((k % 2) * pr, (k // 2) * pc) if wide else (k * pr, 0)
            part[i, k % 2, k // 2] = total[row:row + pr, col:col + pc]
        halves(i).start()

    def halves(i):
        return remote(part.at[i, 1 - c], from_sib.at[i], hs.at[i], hr.at[i], (f, t ^ 1))

    def spread(i, k):
        return remote(wire.at[i, k], landed.at[i, k], ws.at[i, k], wr.at[i, k], (f, 2 * (z ^ k) + c))

    def scatter(u):
        i = u[0] * subs + u[1]
        halves(i).wait_recv()
        for k in range(nz - 1, 0, -1):
            wire[i, k] = (part[i, c, z ^ k] + from_sib[i, z ^ k]).astype(BF16)
            spread(i, k).start()

    def trade(u):
        i = u[0] * subs + u[1]
        return remote(final.at[i], got.at[u[1], f, t], ts.at[i], tr.at[i], (f ^ u[0], t))

    def traded(u):
        i = u[0] * subs + u[1]
        spot = got.at[u[1], f ^ u[0], t]
        return remote(spot, spot, ts.at[i], tr.at[i], (f ^ u[0], t))

    def finish(u):
        m, h = u
        i = m * subs + h
        value = part[i, c, z] + from_sib[i, z]
        for k in range(1, nz):
            spread(i, k).wait_recv()
            value = value + landed[i, k].astype(F32)
        if m == 0:
            got[h, f, t] = value.astype(BF16)
        else:
            final[i] = value.astype(BF16)
            trade(u).start()

    def ahead(u, k):
        i = u[0] * subs + u[1]
        spot = got.at[u[1], f ^ u[0], t]
        return remote(spot, spot, gs.at[i, k], gr.at[i, k], (f, t ^ (2 * k)))

    def came(u, k):
        i = u[0] * subs + u[1]
        spot = got.at[u[1], f ^ u[0], t ^ (2 * k)]
        return remote(spot, spot, gs.at[i, k], gr.at[i, k], (f, t ^ (2 * k)))

    def over(u, k, mine=True):
        i = u[0] * subs + u[1]
        spot = got.at[u[1], f ^ u[0], (t if mine else t ^ 1) ^ (2 * k)]
        return remote(spot, spot, ks.at[i, k], kr.at[i, k], (f, t ^ 1))

    def announce(u):
        if u[0]:
            traded(u).wait_recv()
        for k in range(nz - 1, 0, -1):
            ahead(u, k).start()
        over(u, 0).start()

    def relay(u):
        for k in range(1, nz):
            came(u, k).wait_recv()
            over(u, k).start()

    def down(m, first):
        g = f ^ m
        value = contract_first(sqr[g], cot_all[g, :, own_cols])
        dgrad[...] = value if first else dgrad[...] + value

    def up_part(m, first):
        g = f ^ m
        value = contract_first(inp_all[g], pre[g])
        ugrad[...] = value if first else ugrad[...] + value

    single = lambda p: p[0] in singles
    near = [p for p in inner if single(p)] + [p for p in outer if single(p)]
    far = [p for p in pairs if not single(p)]
    ahead_k = [k for k in zorder if rings[masks[0], 0].targets(0, k)]
    end_k = [k for k in zorder if k not in ahead_k]
    spots = lambda items: [p for p in items if p[1] < strips]
    near_spots, far_spots = spots(near), spots(far)

    g_cot.push_own()
    g_dw.push_own((0,))
    take_cot(near)
    g_dw.push_own((1,))
    for m, s in near_spots[:2]:
        turn(m, s, ahead_k)
    take(g_dw, inner)
    g_pa.push_own()
    take_cot(far)
    for m, s in near_spots[2:]:
        turn(m, s, ahead_k)
    for m, s in near_spots:
        turn(m, s, end_k)
    for m, s in far_spots:
        turn(m, s, ahead_k)
    take(g_dw, outer)
    for copy in own:
        copy.wait()

    middle = [p for p in outer if single(p)]
    last = [p for p in outer if not single(p)]
    pieces = inner, middle, last
    if subs == 1:
        inner, middle, last = [], [(m, 0) for m in singles], [(m, 0) for m in masks if m not in singles]
    first_units = [(0, h) for h in range(subs)]
    square_grad(0)
    for u in first_units:
        unit(u)
    for m, s in far_spots:
        turn(m, s, end_k)
    square_grad(singles[0])
    for u in first_units:
        scatter(u)
    for m in singles[1:]:
        square_grad(m)
    for u in first_units:
        finish(u)
        announce(u)

    def come(items):
        for m, cls in items:
            g_pa.arrive(cls, m)

    def forward(items):
        for m, cls in items:
            g_pa.push(cls, m)

    come(pieces[0])
    if subs == 1:
        forward(pieces[0])
    for u in inner:
        unit(u)
    for m in masks:
        if m not in singles:
            square_grad(m)
    for u in inner:
        scatter(u)
    down(0, True)
    for u in first_units:
        relay(u)
    up_part(0, True)
    for u in inner:
        finish(u)
    if subs == 2:
        forward(pieces[0])
    take(g_pa, pieces[1])
    for u in middle:
        unit(u)
    for u in inner:
        announce(u)
    for u in middle:
        scatter(u)
    for m in singles:
        down(m, False)
    for u in middle:
        finish(u)
    for m in masks:
        exchange(m).start()
    for u in inner:
        relay(u)
    for p, u in zip(pieces[2], last) if subs == 2 else []:
        come([p])
        unit(u)
    if subs == 1:
        take(g_pa, pieces[2])
        for u in last:
            unit(u)
    for u in last:
        scatter(u)
    for u in middle:
        announce(u)
    for m in masks:
        if m not in singles:
            down(m, False)
    dn_own[...] = jnp.sum(dgrad[...] * dgrad[...], axis=1).reshape(1, ff)
    for u in last:
        finish(u)
    downs = [remote(dn_own, dn_all.at[f], ds.at[m], dr.at[m], (f ^ m, t)) for m in range(1, nf)]
    for copy in downs:
        copy.start()
    for m in masks:
        exchanged(m).wait_recv()
        in_to(m).start()
    for u in last:
        announce(u)
    for u in middle:
        relay(u)
    for m in masks:
        in_from(m).wait_recv()
        up_part(m, False)
    un_own[...] = jnp.sum(ugrad[...] * ugrad[...], axis=1).reshape(1, db)
    ups = [remote(un_own, un_all.at[t], us.at[m], ur.at[m], (f, t ^ m)) for m in range(1, nt)]
    for copy in ups:
        copy.start()
    for u in last:
        relay(u)

    dn_all[f] = dn_own[...]
    un_all[t] = un_own[...]
    for m in range(1, nf):
        remote(dn_all.at[f ^ m], dn_all.at[f ^ m], ds.at[m], dr.at[m], (f ^ m, t)).wait_recv()
    for m in range(1, nt):
        remote(un_all.at[t ^ m], un_all.at[t ^ m], us.at[m], ur.at[m], (f, t ^ m)).wait_recv()
    units = first_units + inner + middle + last
    for u in units:
        for k in range(nz):
            over(u, k, False).wait_recv()

    for u in units:
        i = u[0] * subs + u[1]
        halves(i).wait_send()
        for k in range(1, nz):
            spread(i, k).wait_send()
            ahead(u, k).wait_send()
        for k in range(nz):
            over(u, k).wait_send()
        if u[0]:
            trade(u).wait_send()
    for m in masks:
        for s in range(strips):
            for k in range(nz):
                to_sibling(m, s, k).wait_send()
            rings[m, s].drain()
        in_to(m).wait_send()
        exchange(m).wait_send()
    for g in (g_cot, g_dw, g_pa):
        g.drain()
    for copy in ups + downs:
        copy.wait_send()


def fused(nf, nt, cot, dw, pa, inp, up):
    rows, d = inp.shape
    ff, db = dw.shape
    nz = nt // 2
    subs = strips = 2 if nf * nz <= 64 else 1
    half = rows // subs
    pr, pc = piece_shape(nt, half, db)
    units = nf * subs
    dma = pltpu.SemaphoreType.DMA
    vmem = pl.BlockSpec(memory_space=pltpu.VMEM)
    hbm = pl.BlockSpec(memory_space=pl.ANY)
    V = pltpu.VMEM
    sems = [dma((3, 2, nf))] * 2 + [dma((nf, strips, nz))] * 4 + [dma((nf,))] * 4
    sems += [dma((units,))] * 2 + [dma((units, nz))] * 2 + [dma((units,))] * 2 + [dma((units, nz))] * 4
    sems += [dma((nt,))] * 2 + [dma((nf,))] * 2 + [dma((6,))]
    return pl.pallas_call(
        functools.partial(fused_kernel, nf, nt, subs, strips),
        out_shape=[
            V((db, ff), F32), V((ff, db), F32), V((subs, nf, nt, pr, pc), BF16),
            V((nt, 1, db), F32), V((nf, 1, ff), F32),
        ],
        in_specs=[hbm] * 5,
        out_specs=[vmem] * 5,
        scratch_shapes=[
            V((nf, rows, d), BF16), V((ff, d), BF16), V((nf, rows, ff), BF16), V((nf, rows, db), BF16),
            V((db, ff), BF16), V((nf, rows, ff), BF16), V((nf, rows, ff), BF16), V((nf, rows, ff), F32),
            V((units, 2, nz, pr, pc), F32), V((units, nz, pr, pc), F32),
            V((units, nz, pr, pc), BF16), V((units, nz, pr, pc), BF16), V((units, pr, pc), BF16),
            V((1, db), F32), V((1, ff), F32),
        ] + sems,
        compiler_params=pltpu.CompilerParams(has_side_effects=True, collective_id=0, vmem_limit_bytes=54 * 2 ** 20),
    )(cot, dw, pa, inp, up)


def deliver_kernel(ugrad, dgrad, got, un_all, dn_all, ug_out, dg_out, out, un_out, dn_out, whole, un_sum, dn_sum, sem):
    subs, nf, nt, pr, pc = got.shape
    rows, d = whole.shape
    half, db = rows // subs, d // nf
    copies = [pltpu.make_async_copy(ugrad, ug_out, sem.at[0]), pltpu.make_async_copy(dgrad, dg_out, sem.at[1])]
    for copy in copies:
        copy.start()
    wide = half // 2 == pr
    for h in range(subs):
        for k in range(nt):
            for g in range(nf):
                row, col = ((k % 2) * pr, (k // 2) * pc) if wide else (k * pr, 0)
                whole[h * half + row:h * half + row + pr, g * db + col:g * db + col + pc] = got[h, g, k]
    un, dn = un_all[0], dn_all[0]
    for k in range(1, nt):
        un = un + un_all[k]
    for k in range(1, nf):
        dn = dn + dn_all[k]
    un_sum[...] = un
    dn_sum[...] = dn
    last = [pltpu.make_async_copy(whole, out, sem.at[2]), pltpu.make_async_copy(un_sum, un_out, sem.at[3]),
            pltpu.make_async_copy(dn_sum, dn_out, sem.at[4])]
    for copy in last:
        copy.start()
    for copy in copies + last:
        copy.wait()


def deliver(rows, d, ugrad, dgrad, got, un_all, dn_all):
    hbm, vmem = pl.BlockSpec(memory_space=pl.ANY), pl.BlockSpec(memory_space=pltpu.VMEM)
    V = pltpu.VMEM
    un, dn = un_all.shape[1:], dn_all.shape[1:]
    H = jax.ShapeDtypeStruct
    return pl.pallas_call(
        deliver_kernel,
        out_shape=[H(ugrad.shape, F32), H(dgrad.shape, F32), H((rows, d), BF16), H(un, F32), H(dn, F32)],
        in_specs=[vmem] * 5,
        out_specs=[hbm] * 5,
        scratch_shapes=[V((rows, d), BF16), V(un, F32), V(dn, F32), pltpu.SemaphoreType.DMA((5,))],
        compiler_params=pltpu.CompilerParams(vmem_limit_bytes=16 * 2 ** 20),
    )(ugrad, dgrad, got, un_all, dn_all)


def local(nf, nt, inputs, pre_act, cotangent, up_weight, down_weight):
    db, ff = up_weight.shape
    parts = fused(nf, nt, cotangent, down_weight, pre_act, inputs, up_weight)
    up_grad, down_grad, out, un, dn = deliver(*inputs.shape, *parts)
    return out, up_grad, down_grad, un.reshape(db), dn.reshape(ff)


def solution(mesh):
    in_specs = (P("fs", None), P("fs", "tp"), P("fs", None), P("fs", "tp"), P("tp", "fs"))
    out_specs = (P("fs", None), P("fs", "tp"), P("tp", "fs"), P("fs"), P("tp"))
    body = functools.partial(local, mesh.shape["fs"], mesh.shape["tp"])
    return jax.shard_map(body, mesh=mesh, in_specs=in_specs, out_specs=out_specs, check_vma=False)
```

profile of v0, /device:TPU:0, one launch (start us, length us, event | category | flops | bytes accessed | tf_op | source)
XLA Modules:
  0.0 102.6 jit_solution(16347316257344273421)
XLA Ops:
  0.6 99.3 %shard_map.92 = (f32[512,1024]{1,0:T(8,128)S(1)}, f32[1024,512]{1,0:T(8,128)S(1)}, bf16[2,4,8,96,128]{4,3,2,1,0:T(8,128)(2,1)S(1)}, f32[8,1,512]{2,1,0:T(1,128)S(1)}, f32[4,1,1024]{2,1,0:T(1,128)S(1)}) custom-call(bf16[384,2048]{1,0:T(8,128)(2,1)} %cot.1, bf16[1024,512]{1,0:T(8,128)(2,1)} %dw.1, bf16[384,1024]{1,0:T(8,128)(2,1)} %pa.1, ...), custom_call_target="tpu_custom_call" | custom-call | tf_op jit(solution)/shard_map/pallas_call | solution.py:492
  99.9 2.6 %shard_map.93 = (f32[512,1024]{1,0:T(8,128)}, f32[1024,512]{1,0:T(8,128)}, bf16[384,2048]{1,0:T(8,128)(2,1)}, f32[1,512]{1,0:T(1,128)}, f32[1,1024]{1,0:T(1,128)}) custom-call(f32[512,1024]{1,0:T(8,128)S(1)} %get-tuple-element.15.ugrad, f32[1024,512]{1,0:T(8,128)S(1)} %get-tuple-element.16.dgrad, bf16[2,4,8,96,128]{4,3,2,1,0:T(8,128)(2,1)S(1)} %get-tuple-element.17.got, ...), custom_call_target="tpu_custom_call" | custom-call | tf_op jit(solution)/shard_map/pallas_call | solution.py:544
where the time goes:
time: 103 us
  Pallas kernels  102 us (99%)
    pallas_call x1, Pallas kernels, fused(): pl.pallas_call(functools.partial(fused_kernel, nf, nt, subs, strips), out...  99.3 us
    pallas_call x1, Pallas kernels, deliver(): pl.pallas_call(deliver_kernel, out_shape=[H(ugrad.shape, F32), H(dgrad.sh...  2.57 us

commit v1 on v0

v1 whole, which is shorter than its diff:
```python
import functools

import jax
import jax.numpy as jnp
from jax import lax
from jax.experimental import pallas as pl
from jax.experimental.pallas import tpu as pltpu
from jax.sharding import PartitionSpec as P

MESH = pl.DeviceIdType.MESH
F32, BF16 = jnp.float32, jnp.bfloat16


def contract_last(left, right):
    return lax.dot_general(left, right, (((1,), (1,)), ((), ())), preferred_element_type=F32)


def contract_first(left, right):
    return lax.dot_general(left, right, (((0,), (0,)), ((), ())), preferred_element_type=F32)


def bits_of(n):
    return [1 << i for i in range(n.bit_length() - 1)]


def by_weight(n, down=False):
    return sorted(range(1, n), key=lambda m: (bin(m).count("1"), -m if down else m))


class Gather:
    def __init__(self, n, me, device, source, place, send, recv, orders):
        self.n, self.me, self.device = n, me, device
        self.source, self.place = source, place
        self.send, self.recv, self.orders = send, recv, orders

    def targets(self, cls, m):
        bits = bits_of(self.n)
        if self.orders[cls] == "flat":
            return list(range(self.n - 1, 0, -1)) if m == 0 else []
        if m == 0:
            return bits
        if self.orders[cls] == "up":
            return [b for b in bits if b > m]
        return [b for b in bits if b < (m & -m)]

    def copy(self, cls, m, b):
        there = self.place(self.me ^ m, cls)
        return pltpu.make_async_remote_copy(
            src_ref=self.source(cls) if m == 0 else there,
            dst_ref=there,
            send_sem=self.send,
            recv_sem=self.recv(cls, m ^ b),
            device_id=self.device(self.me ^ b),
            device_id_type=MESH,
        )

    def push(self, cls, m, only=None):
        for b in self.targets(cls, m):
            if only is None or b == only:
                self.copy(cls, m, b).start()

    def push_own(self, turns=None):
        classes = list(range(len(self.orders)))
        for i, b in enumerate(bits_of(self.n)):
            for j, cls in enumerate(classes if i % 2 == 0 else classes[::-1]):
                if turns is None or j in turns:
                    self.push(cls, 0, b)

    def arrive(self, cls, m):
        here = self.place(self.me ^ m, cls)
        pltpu.make_async_remote_copy(
            src_ref=here,
            dst_ref=here,
            send_sem=self.send,
            recv_sem=self.recv(cls, m),
            device_id=self.device(self.me ^ (m & -m)),
            device_id_type=MESH,
        ).wait_recv()

    def drain(self, sent):
        pltpu.make_async_remote_copy(src_ref=sent, dst_ref=sent, send_sem=self.send, recv_sem=self.send,
                                     device_id=self.device(self.me ^ 1), device_id_type=MESH).wait_send()


def share_rows(rows, parts):
    cuts = 1
    while cuts < parts and rows % (2 * cuts * 16) == 0:
        cuts *= 2
    return cuts


def piece_shape(nt, rows, db):
    nz = nt // 2
    if db % (128 * nz) == 0:
        return rows // 2, db // nz
    return rows // nt, db


def fused_kernel(nf, nt, subs, strips, cot, dw, pa, inp, up, ugrad, dgrad, got, un_all, dn_all,
                 cot_all, dw_all, pa_all, inp_all, up_all, pre, sqr, sq,
                 part, from_sib, wire, landed, final, un_own, dn_own,
                 xs, xr, pa_r, zs, zr, ss, sr, a_s, a_r, bs, br, hs, hr, ws, wr, ts, tr, gs, gr, ks, kr,
                 us, ur, ds, dr, local_sem):
    f, t = lax.axis_index("fs"), lax.axis_index("tp")
    z, c = t // 2, t % 2
    nz = nt // 2
    rows, d = cot.shape
    ff, db = dw.shape
    height = rows // subs
    pr, pc = part.shape[3:]
    own_cols = pl.ds(pl.multiple_of(f * db, db), db)

    def remote(src, dst, send, recv, device):
        return pltpu.make_async_remote_copy(src_ref=src, dst_ref=dst, send_sem=send, recv_sem=recv,
                                            device_id=device, device_id_type=MESH)

    ih = rows // 2

    def columns(g, side):
        return inp.at[pl.ds(pl.multiple_of(side * ih, ih), ih), pl.ds(pl.multiple_of(g * db, db), db)]

    def in_half(g, side):
        return inp_all.at[g, pl.ds(pl.multiple_of(side * ih, ih), ih), :]

    own = [
        pltpu.make_async_copy(cot, cot_all.at[f], local_sem.at[0]),
        pltpu.make_async_copy(dw, dw_all.at[:, own_cols], local_sem.at[1]),
        pltpu.make_async_copy(pa, pa_all.at[f], local_sem.at[2]),
        pltpu.make_async_copy(up, up_all, local_sem.at[3]),
        pltpu.make_async_copy(inp.at[:, own_cols], inp_all.at[f], local_sem.at[4]),
    ]
    for copy in own:
        copy.start()

    barrier = pltpu.get_barrier_semaphore()
    peers = [(f ^ m, t) for m in range(1, nf)] + [(f, t ^ m) for m in range(1, nt)]
    for peer in peers:
        pl.semaphore_signal(barrier, inc=1, device_id=peer, device_id_type=MESH)
    pl.semaphore_wait(barrier, len(peers))

    row_cuts = share_rows(rows, nt)
    col_cuts = nt // row_cuts
    cr, cc = rows // row_cuts, d // col_cuts

    def piece(ref, y, h=None):
        row = pl.multiple_of((y // col_cuts) * cr, cr)
        width = cc if h is None else cc // 2
        col = (y % col_cuts) * cc + (0 if h is None else h * width)
        return ref.at[pl.ds(row, cr), pl.ds(pl.multiple_of(col, width), width)]

    dwh = ff // 2
    lanes = max(subs, 2)
    pah = rows // lanes

    def over_fs(k, source, place, n=2):
        return Gather(nf, f, lambda g: (g, t), source, place, xs.at[k],
                      lambda cls, m: pa_r.at[cls, m - 1] if k == 2 else xr.at[k, cls, m - 1],
                      ("up",) * (n // 2) + ("down",) * (n // 2))

    g_cot = over_fs(0, lambda h: piece(cot_all.at[f], t, h), lambda g, h: piece(cot_all.at[g], t, h))
    g_dw = over_fs(1, lambda h: dw_all.at[pl.ds(h * dwh, dwh), own_cols],
                   lambda g, h: dw_all.at[pl.ds(h * dwh, dwh), pl.ds(pl.multiple_of(g * db, db), db)])
    g_pa = over_fs(2, lambda h: pa_all.at[f, pl.ds(h * pah, pah), :],
                   lambda g, h: pa_all.at[g, pl.ds(h * pah, pah), :], lanes)

    def strip(m, s, y):
        return piece(cot_all.at[f ^ m], y, s if strips == 2 else None)

    def over_z(m, s):
        spot = lambda y, cls=0: strip(m, s, 2 * y + c)
        return Gather(nz, z, lambda y: (f, 2 * y + c), lambda cls: spot(z), spot,
                      zs.at[m - 1, s], lambda cls, k: zr.at[m - 1, s, k - 1], ("down",))

    def to_sibling(m, s, k):
        spot = strip(m, s, 2 * (z ^ k) + c)
        return remote(spot, spot, ss.at[m - 1], sr.at[m - 1], (f, t ^ 1))

    def from_sibling(m):
        spot = cot_all.at[pl.ds(0, nz), pl.ds(0, cr), pl.ds(0, cc)]
        return remote(spot, spot, ss.at[m - 1], sr.at[m - 1], (f, t ^ 1))

    exchange = lambda m: remote(columns(f ^ m, c), in_half(f, c), a_s, a_r.at[m - 1], (f ^ m, t))
    exchanged = lambda m: remote(in_half(f ^ m, c), in_half(f ^ m, c), a_s, a_r.at[m - 1], (f ^ m, t))
    in_to = lambda m: remote(in_half(f ^ m, c), in_half(f ^ m, c), bs, br.at[m - 1], (f, t ^ 1))
    in_from = lambda m: remote(in_half(f ^ m, 1 - c), in_half(f ^ m, 1 - c), bs, br.at[m - 1], (f, t ^ 1))

    masks = by_weight(nf)
    zorder = by_weight(nz, True)
    left = {m: 2 for m in masks}
    rings = {(m, s): over_z(m, s) for m in masks for s in range(strips)}
    singles = [m for m in masks if m & (m - 1) == 0]
    pairs = [(m, cls) for m in masks for cls in (0, 1)]
    inner = [p for p in pairs if g_dw.targets(p[1], p[0])]
    outer = [p for p in pairs if p not in inner]

    def take_cot(items):
        for m, cls in items:
            g_cot.arrive(cls, m)
            g_cot.push(cls, m)
            left[m] -= 1
            if strips == 2:
                rings[m, cls].push(0, 0)
                to_sibling(m, cls, 0).start()
            elif left[m] == 0:
                rings[m, 0].push(0, 0)
                to_sibling(m, 0, 0).start()

    def turn(m, s, steps):
        for k in steps:
            rings[m, s].arrive(0, k)
            rings[m, s].push(0, k)
            to_sibling(m, s, k).start()

    def take(g, items):
        for m, cls in items:
            g.arrive(cls, m)
            g.push(cls, m)

    tile = min(ff, 256)

    def square_grad(m):
        g = f ^ m
        if m:
            from_sibling(m).wait_recv()
        sq[g] = contract_last(cot_all[g], dw_all[...])

    def unit(u):
        m, q, n = u
        g = f ^ m
        i = m * subs + q
        some = pl.ds(q * height, n * height)
        for j in range(ff // tile):
            cols = pl.ds(j * tile, tile)
            active = jnp.maximum(pa_all[g, some, cols].astype(F32), 0.0)
            pre[g, some, cols] = (2.0 * active * sq[g, some, cols]).astype(BF16)
            sqr[g, some, cols] = (active * active).astype(BF16)
        total = contract_last(pre[g, some, :], up_all[...])
        for e in range(n):
            for k in range(nt):
                row, col = ((k % 2) * pr, (k // 2) * pc) if wide else (k * pr, 0)
                row += e * height
                part[k % 2, k // 2, i + e] = total[row:row + pr, col:col + pc]
        halves(u).start()

    wide = height // 2 == pr
    first_slot = lambda u: every.index(u)
    slots = lambda u: pl.ds(u[0] * subs + u[1], u[2])

    def halves(u):
        i = first_slot(u)
        return remote(part.at[1 - c, :, slots(u)], from_sib.at[:, slots(u)], hs.at[i], hr.at[i], (f, t ^ 1))

    def spread(u, k):
        i = first_slot(u)
        return remote(wire.at[k, slots(u)], landed.at[k, slots(u)], ws.at[i], wr.at[i], (f, 2 * (z ^ k) + c))

    def spreads(u):
        i = first_slot(u)
        return remote(wire.at[pl.ds(1, nz - 1), slots(u)], landed.at[pl.ds(1, nz - 1), slots(u)],
                      ws.at[i], wr.at[i], (f, t ^ 2))

    def scatter(u):
        halves(u).wait_recv()
        for k in range(nz - 1, 0, -1):
            wire[k, slots(u)] = (part[c, z ^ k, slots(u)] + from_sib[z ^ k, slots(u)]).astype(BF16)
            spread(u, k).start()

    def home(u, g, k):
        return got.at[g, k, pl.ds(u[1], u[2])]

    def trade(u):
        i = first_slot(u)
        return remote(final.at[slots(u)], home(u, f, t), ts.at[i], tr.at[i], (f ^ u[0], t))

    def traded(u):
        i = first_slot(u)
        spot = home(u, f ^ u[0], t)
        return remote(spot, spot, ts.at[i], tr.at[i], (f ^ u[0], t))

    def finish(u):
        value = part[c, z, slots(u)] + from_sib[z, slots(u)]
        spreads(u).wait()
        for k in range(1, nz):
            value = value + landed[k, slots(u)].astype(F32)
        halves(u).wait_send()
        if u[0] == 0:
            got[f, t, pl.ds(u[1], u[2])] = value.astype(BF16)
        else:
            final[slots(u)] = value.astype(BF16)
            trade(u).start()

    def ring_of(u):
        i = first_slot(u)
        spot = lambda y, cls=0: home(u, f ^ u[0], 2 * y + c)
        return Gather(nz, z, lambda y: (f, 2 * y + c), lambda cls: spot(z), spot,
                      gs.at[i], lambda cls, k: gr.at[i, k - 1],
                      ("flat",) if u in late else ("down",))

    def over(u, k):
        spot = home(u, f ^ u[0], t ^ (2 * k))
        i = first_slot(u)
        return remote(spot, spot, ks.at[i], kr.at[i], (f, t ^ 1))

    def overs(u):
        i = first_slot(u)
        spot = landed.at[:, slots(u)]
        return remote(spot, spot, ks.at[i], kr.at[i], (f, t ^ 1))

    def announce(u):
        if u[0]:
            traded(u).wait_recv()
        outs[u] = ring_of(u)
        outs[u].push(0, 0)
        over(u, 0).start()

    def pass_on(u, steps):
        for k in steps:
            outs[u].arrive(0, k)
            outs[u].push(0, k)
            over(u, k).start()

    def down(m, first):
        g = f ^ m
        value = contract_first(sqr[g], cot_all[g, :, own_cols])
        dgrad[...] = value if first else dgrad[...] + value

    def up_part(m, first):
        g = f ^ m
        value = contract_first(inp_all[g], pre[g])
        ugrad[...] = value if first else ugrad[...] + value

    single = lambda p: p[0] in singles
    near = [p for p in inner if single(p)] + [p for p in outer if single(p)]
    far = [p for p in pairs if not single(p)]
    ahead_k = [k for k in zorder if rings[masks[0], 0].targets(0, k)]
    end_k = [k for k in zorder if k not in ahead_k]
    spots = lambda items: [p for p in items if p[1] < strips]
    near_spots, far_spots = spots(near), spots(far)

    own[0].wait()
    g_cot.push_own()
    own[1].wait()
    g_dw.push_own((0,))
    take_cot(near)
    g_dw.push_own((1,))
    for m, s in near_spots[:2]:
        turn(m, s, ahead_k)
    take(g_dw, inner)
    own[2].wait()
    g_pa.push_own()
    take_cot(far)
    for m, s in near_spots[2:]:
        turn(m, s, ahead_k)
    for m, s in near_spots:
        turn(m, s, end_k)
    for m, s in far_spots:
        turn(m, s, ahead_k)
    take(g_dw, outer)
    for copy in own[3:]:
        copy.wait()

    heads = [(m, q) for j in range(lanes // 2) for q in (j, lanes - 1 - j) for m in masks]
    inner = [p for p in heads if g_pa.targets(p[1], p[0])]
    middle = [p for p in heads if p not in inner and single(p)]
    last = [p for p in heads if p not in inner and not single(p)]
    first_units = [(0, 0, subs)]
    if subs == 1:
        inner_units, middle_units = [], [(m, 0, 1) for m in singles]
        last_units = [(m, 0, 1) for m in masks if m not in singles]
    else:
        side = lanes // 2
        inner_units = [(m, q, side) for m in masks for q in (0, side) if (m, q) in inner]
        middle_units = [(m, q, side) for m in masks for q in (0, side) if (m, q) in middle]
        last_units = [(m, q, 1) for m, q in last]
    early, late = last_units[:len(last_units) // 2], last_units[len(last_units) // 2:]
    outs = {}
    every = first_units + inner_units + middle_units + last_units
    square_grad(0)
    for u in first_units:
        unit(u)
    for m, s in far_spots:
        turn(m, s, end_k)
    square_grad(singles[0])
    for u in first_units:
        scatter(u)
    for m in masks[1:]:
        square_grad(m)

    def come(items):
        for m, cls in items:
            g_pa.arrive(cls, m)

    def forward(items):
        for m, cls in items:
            g_pa.push(cls, m)

    def settle():
        width = cc // strips
        for m in masks:
            from_sibling(m).wait_send()
            for s in range(strips):
                rings[m, s].drain(cot_all.at[pl.ds(0, nz - 1), pl.ds(0, cr), pl.ds(0, width)])
        g_cot.drain(cot_all.at[pl.ds(0, nf - 1), pl.ds(0, cr), pl.ds(0, cc)])
        g_dw.drain(dw_all.at[:, pl.ds(0, (nf - 1) * db)])

    come(inner)
    forward(inner[:len(inner) // 2])
    for u in inner_units:
        unit(u)
    for u in first_units:
        finish(u)
    for u in inner_units:
        scatter(u)
    for u in first_units:
        announce(u)
    settle()
    down(0, True)
    up_part(0, True)
    for u in inner_units:
        finish(u)
    forward(inner[len(inner) // 2:])
    for m in masks:
        if m not in singles:
            exchange(m).start()
    for u in first_units:
        pass_on(u, ahead_k)
    take(g_pa, middle)
    for u in middle_units:
        unit(u)
    for u in middle_units:
        scatter(u)
    for u in first_units:
        pass_on(u, end_k)
    for u in inner_units:
        announce(u)
    for m in singles:
        down(m, False)

    def final_units(items):
        for u in items:
            if subs > 1:
                come([(u[0], u[1])])
            unit(u)
        for u in items:
            scatter(u)

    if subs == 1:
        take(g_pa, last)
    final_units(early)
    for u in middle_units:
        finish(u)
    for m in singles:
        exchange(m).start()
    final_units(late)
    for u in inner_units:
        pass_on(u, ahead_k)
    for u in middle_units:
        announce(u)
    for u in inner_units:
        pass_on(u, end_k)
    for u in early:
        finish(u)
    for m in masks:
        if m not in singles:
            down(m, False)
    for u in late:
        finish(u)
    dn_own[...] = jnp.sum(dgrad[...] * dgrad[...], axis=1).reshape(1, ff)
    downs = [remote(dn_own, dn_all.at[f], ds, dr, (f ^ m, t)) for m in range(1, nf)]
    for copy in downs:
        copy.start()

    def swap_in(items):
        for m in items:
            exchanged(m).wait_recv()
            in_to(m).start()

    swap_in([m for m in masks if m not in singles])
    for u in early:
        announce(u)
    for u in middle_units:
        pass_on(u, ahead_k)
    for u in late:
        announce(u)
    swap_in(singles)
    for m in masks[::-1]:
        in_from(m).wait_recv()
        up_part(m, False)
    un_own[...] = jnp.sum(ugrad[...] * ugrad[...], axis=1).reshape(1, db)
    ups = [remote(un_own, un_all.at[t], us, ur, (f, t ^ m)) for m in range(1, nt)]
    for copy in ups:
        copy.start()
    for u in early:
        pass_on(u, ahead_k)
    for u in middle_units + early:
        pass_on(u, end_k)
    for u in late:
        pass_on(u, zorder)

    def up_sums():
        spot = un_all.at[pl.ds(0, nt - 1)]
        return remote(spot, spot, us, ur, (f, t ^ 1))

    def down_sums():
        spot = dn_all.at[pl.ds(0, nf - 1)]
        return remote(spot, spot, ds, dr, (f ^ 1, t))

    def norms_in():
        dn_all[f] = dn_own[...]
        un_all[t] = un_own[...]
        down_sums().wait_recv()
        up_sums().wait_recv()

    norms_in()

    def gathered():
        for u in every:
            overs(u).wait_recv()

    def drain():
        for u in every:
            outs[u].drain(landed.at[pl.ds(1, nz - 1), slots(u)])
            overs(u).wait_send()
            if u[0]:
                trade(u).wait_send()
        spot = inp_all.at[pl.ds(0, nf - 1), pl.ds(0, ih)]
        remote(spot, spot, a_s, bs, (f, t ^ 1)).wait_send()
        remote(spot, spot, bs, a_s, (f, t ^ 1)).wait_send()
        g_pa.drain(pa_all.at[pl.ds(0, nf - 1)])
        up_sums().wait_send()
        down_sums().wait_send()

    gathered()
    drain()


def fused(nf, nt, cot, dw, pa, inp, up):
    rows, d = inp.shape
    ff, db = dw.shape
    nz = nt // 2
    subs, strips = (4, 2) if nf * nz <= 64 else (1, 1)
    half = rows // subs
    pr, pc = piece_shape(nt, half, db)
    units = nf * subs
    dma = pltpu.SemaphoreType.DMA
    vmem = pl.BlockSpec(memory_space=pltpu.VMEM)
    hbm = pl.BlockSpec(memory_space=pl.ANY)
    V = pltpu.VMEM
    n = nf - 1
    count = 9 if subs == 4 and nf == 4 else nf
    sems = [dma((3,)), dma((2, 2, n)), dma((max(subs, 2), n)), dma((n, strips)), dma((n, strips, nz - 1))]
    sems += [dma((n,)), dma((n,)), dma(()), dma((n,)), dma(()), dma((n,))] + [dma((count,))] * 7
    sems += [dma((count, nz - 1)), dma((count,)), dma((count,)), dma(()), dma(()), dma(()), dma(()), dma((5,))]
    return pl.pallas_call(
        functools.partial(fused_kernel, nf, nt, subs, strips),
        out_shape=[
            V((db, ff), F32), V((ff, db), F32), V((nf, nt, subs, pr, pc), BF16),
            V((nt, 1, db), F32), V((nf, 1, ff), F32),
        ],
        in_specs=[hbm] * 5,
        out_specs=[vmem] * 5,
        scratch_shapes=[
            V((nf, rows, d), BF16), V((ff, d), BF16), V((nf, rows, ff), BF16), V((nf, rows, db), BF16),
            V((db, ff), BF16), V((nf, rows, ff), BF16), V((nf, rows, ff), BF16), V((nf, rows, ff), F32),
            V((2, nz, units, pr, pc), F32), V((nz, units, pr, pc), F32),
            V((nz, units, pr, pc), BF16), V((nz, units, pr, pc), BF16), V((units, pr, pc), BF16),
            V((1, db), F32), V((1, ff), F32),
        ] + sems,
        compiler_params=pltpu.CompilerParams(has_side_effects=True, collective_id=0, vmem_limit_bytes=54 * 2 ** 20),
    )(cot, dw, pa, inp, up)


def deliver_kernel(ugrad, dgrad, got, un_all, dn_all, ug_out, dg_out, out, un_out, dn_out, whole, un_sum, dn_sum, sem):
    nf, nt, subs, pr, pc = got.shape
    rows, d = whole.shape
    half, db = rows // subs, d // nf
    copies = [pltpu.make_async_copy(ugrad, ug_out, sem.at[0]), pltpu.make_async_copy(dgrad, dg_out, sem.at[1])]
    for copy in copies:
        copy.start()
    wide = half // 2 == pr
    for h in range(subs):
        for k in range(nt):
            for g in range(nf):
                row, col = ((k % 2) * pr, (k // 2) * pc) if wide else (k * pr, 0)
                whole[h * half + row:h * half + row + pr, g * db + col:g * db + col + pc] = got[g, k, h]
    un, dn = un_all[0], dn_all[0]
    for k in range(1, nt):
        un = un + un_all[k]
    for k in range(1, nf):
        dn = dn + dn_all[k]
    un_sum[...] = un
    dn_sum[...] = dn
    last = [pltpu.make_async_copy(whole, out, sem.at[2]), pltpu.make_async_copy(un_sum, un_out, sem.at[3]),
            pltpu.make_async_copy(dn_sum, dn_out, sem.at[4])]
    for copy in last:
        copy.start()
    for copy in copies + last:
        copy.wait()


def deliver(rows, d, ugrad, dgrad, got, un_all, dn_all):
    hbm, vmem = pl.BlockSpec(memory_space=pl.ANY), pl.BlockSpec(memory_space=pltpu.VMEM)
    V = pltpu.VMEM
    un, dn = un_all.shape[1:], dn_all.shape[1:]
    H = jax.ShapeDtypeStruct
    return pl.pallas_call(
        deliver_kernel,
        out_shape=[H(ugrad.shape, F32), H(dgrad.shape, F32), H((rows, d), BF16), H(un, F32), H(dn, F32)],
        in_specs=[vmem] * 5,
        out_specs=[hbm] * 5,
        scratch_shapes=[V((rows, d), BF16), V(un, F32), V(dn, F32), pltpu.SemaphoreType.DMA((5,))],
        compiler_params=pltpu.CompilerParams(vmem_limit_bytes=16 * 2 ** 20),
    )(ugrad, dgrad, got, un_all, dn_all)


def local(nf, nt, inputs, pre_act, cotangent, up_weight, down_weight):
    db, ff = up_weight.shape
    parts = fused(nf, nt, cotangent, down_weight, pre_act, inputs, up_weight)
    up_grad, down_grad, out, un, dn = deliver(*inputs.shape, *parts)
    return out, up_grad, down_grad, un.reshape(db), dn.reshape(ff)


def solution(mesh):
    in_specs = (P("fs", None), P("fs", "tp"), P("fs", None), P("fs", "tp"), P("tp", "fs"))
    out_specs = (P("fs", None), P("fs", "tp"), P("tp", "fs"), P("fs"), P("tp"))
    body = functools.partial(local, mesh.shape["fs"], mesh.shape["tp"])
    return jax.shard_map(body, mesh=mesh, in_specs=in_specs, out_specs=out_specs, check_vma=False)
```

time: 103 us -> 97.1 us (0.943)
  Pallas kernels: 102 us -> 96.3 us
    pallas_call x1, Pallas kernels: 99.3 us -> 93.7 us  [fused(): pl.pallas_call(functools.partial(fused_kernel, nf, nt, subs, strips), out...]
where the time goes in v1:
time: 97.1 us; the launch traced here: 96.9 us
  Pallas kernels  96.3 us (99%)
    pallas_call x1, Pallas kernels, fused(): pl.pallas_call(functools.partial(fused_kernel, nf, nt, subs, strips), out...  93.7 us
    pallas_call x1, Pallas kernels, deliver(): pl.pallas_call(deliver_kernel, out_shape=[H(ugrad.shape, F32), H(dgrad.sh...  2.57 us

profile of v1, /device:TPU:0, one launch (start us, length us, event | category | flops | bytes accessed | tf_op | source)
XLA Modules:
  0.0 96.9 jit_solution(17534611931048269859)
XLA Ops:
  0.6 93.7 %shard_map.92 = (f32[512,1024]{1,0:T(8,128)S(1)}, f32[1024,512]{1,0:T(8,128)S(1)}, bf16[4,8,4,48,128]{4,3,2,1,0:T(8,128)(2,1)S(1)}, f32[8,1,512]{2,1,0:T(1,128)S(1)}, f32[4,1,1024]{2,1,0:T(1,128)S(1)}) custom-call(bf16[384,2048]{1,0:T(8,128)(2,1)} %cot.1, bf16[1024,512]{1,0:T(8,128)(2,1)} %dw.1, bf16[384,1024]{1,0:T(8,128)(2,1)} %pa.1, ...), custom_call_target="tpu_custom_call" | custom-call | tf_op jit(solution)/shard_map/pallas_call | solution.py:554
  94.3 2.6 %shard_map.93 = (f32[512,1024]{1,0:T(8,128)}, f32[1024,512]{1,0:T(8,128)}, bf16[384,2048]{1,0:T(8,128)(2,1)}, f32[1,512]{1,0:T(1,128)}, f32[1,1024]{1,0:T(1,128)}) custom-call(f32[512,1024]{1,0:T(8,128)S(1)} %get-tuple-element.15.ugrad, f32[1024,512]{1,0:T(8,128)S(1)} %get-tuple-element.16.dgrad, bf16[4,8,4,48,128]{4,3,2,1,0:T(8,128)(2,1)S(1)} %get-tuple-element.17.got, ...), custom_call_target="tpu_custom_call" | custom-call | tf_op jit(solution)/shard_map/pallas_call | solution.py:606

commit v2 on v1

--- a/solution.py
+++ b/solution.py
@@ -97,7 +97,7 @@
 
 
 def fused_kernel(nf, nt, subs, strips, cot, dw, pa, inp, up, ugrad, dgrad, got, un_all, dn_all,
-                 cot_all, dw_all, pa_all, inp_all, up_all, pre, sqr, sq,
+                 cot_own, inp_own, cot_all, dw_all, pa_all, inp_all, up_all, pre, sqr, sq,
                  part, from_sib, wire, landed, final, un_own, dn_own,
                  xs, xr, pa_r, zs, zr, ss, sr, a_s, a_r, bs, br, hs, hr, ws, wr, ts, tr, gs, gr, ks, kr,
                  us, ur, ds, dr, local_sem):
@@ -122,14 +122,21 @@
     def in_half(g, side):
         return inp_all.at[g, pl.ds(pl.multiple_of(side * ih, ih), ih), :]
 
+    row_cuts = share_rows(rows, nt)
+    col_cuts = nt // row_cuts
+    cr, cc = rows // row_cuts, d // col_cuts
+    first_piece = cot.at[pl.ds(pl.multiple_of((t // col_cuts) * cr, cr), cr),
+                         pl.ds(pl.multiple_of((t % col_cuts) * cc, cc), cc)]
     own = [
-        pltpu.make_async_copy(cot, cot_all.at[f], local_sem.at[0]),
+        pltpu.make_async_copy(first_piece, cot_own, local_sem.at[0]),
         pltpu.make_async_copy(dw, dw_all.at[:, own_cols], local_sem.at[1]),
         pltpu.make_async_copy(pa, pa_all.at[f], local_sem.at[2]),
-        pltpu.make_async_copy(up, up_all, local_sem.at[3]),
-        pltpu.make_async_copy(inp.at[:, own_cols], inp_all.at[f], local_sem.at[4]),
+        pltpu.make_async_copy(cot, cot_all.at[f], local_sem.at[3]),
+        pltpu.make_async_copy(up, up_all, local_sem.at[4]),
+        pltpu.make_async_copy(inp.at[:, own_cols], inp_all.at[f], local_sem.at[5]),
+        pltpu.make_async_copy(inp, inp_own, local_sem.at[6]),
     ]
-    for copy in own:
+    for copy in own[:2]:
         copy.start()
 
     barrier = pltpu.get_barrier_semaphore()
@@ -138,10 +145,6 @@
         pl.semaphore_signal(barrier, inc=1, device_id=peer, device_id_type=MESH)
     pl.semaphore_wait(barrier, len(peers))
 
-    row_cuts = share_rows(rows, nt)
-    col_cuts = nt // row_cuts
-    cr, cc = rows // row_cuts, d // col_cuts
-
     def piece(ref, y, h=None):
         row = pl.multiple_of((y // col_cuts) * cr, cr)
         width = cc if h is None else cc // 2
@@ -157,7 +160,7 @@
                       lambda cls, m: pa_r.at[cls, m - 1] if k == 2 else xr.at[k, cls, m - 1],
                       ("up",) * (n // 2) + ("down",) * (n // 2))
 
-    g_cot = over_fs(0, lambda h: piece(cot_all.at[f], t, h), lambda g, h: piece(cot_all.at[g], t, h))
+    g_cot = over_fs(0, lambda h: cot_own.at[:, pl.ds(h * (cc // 2), cc // 2)], lambda g, h: piece(cot_all.at[g], t, h))
     g_dw = over_fs(1, lambda h: dw_all.at[pl.ds(h * dwh, dwh), own_cols],
                    lambda g, h: dw_all.at[pl.ds(h * dwh, dwh), pl.ds(pl.multiple_of(g * db, db), db)])
     g_pa = over_fs(2, lambda h: pa_all.at[f, pl.ds(h * pah, pah), :],
@@ -179,12 +182,40 @@
         spot = cot_all.at[pl.ds(0, nz), pl.ds(0, cr), pl.ds(0, cc)]
         return remote(spot, spot, ss.at[m - 1], sr.at[m - 1], (f, t ^ 1))
 
-    exchange = lambda m: remote(columns(f ^ m, c), in_half(f, c), a_s, a_r.at[m - 1], (f ^ m, t))
-    exchanged = lambda m: remote(in_half(f ^ m, c), in_half(f ^ m, c), a_s, a_r.at[m - 1], (f ^ m, t))
-    in_to = lambda m: remote(in_half(f ^ m, c), in_half(f ^ m, c), bs, br.at[m - 1], (f, t ^ 1))
-    in_from = lambda m: remote(in_half(f ^ m, 1 - c), in_half(f ^ m, 1 - c), bs, br.at[m - 1], (f, t ^ 1))
+    iq = rows // 4
+    seat = lambda y: (2 * y + c)
+
+    def quarter(g, q):
+        return inp_all.at[g, pl.ds(pl.multiple_of(q * iq, iq), iq), :]
+
+    def source(m):
+        height, q = (iq, seat(z % 2)) if m == deep_m else (ih, c)
+        return inp_own.at[pl.ds(pl.multiple_of(q * height, height), height), pl.ds(pl.multiple_of((f ^ m) * db, db), db)]
+
+    def place(m, g):
+        return quarter(g, seat(z % 2)) if m == deep_m else in_half(g, c)
+
+    exchange = lambda m: remote(source(m), place(m, f), a_s.at[m - 1], a_r.at[m - 1], (f ^ m, t))
+    exchanged = lambda m: remote(place(m, f ^ m), place(m, f ^ m), a_s.at[m - 1], a_r.at[m - 1], (f ^ m, t))
+    in_to = lambda m: remote(place(m, f ^ m), place(m, f ^ m), bs.at[m - 1], br.at[m - 1], (f, t ^ 1))
+
+    def in_from(m):
+        return remote(in_half(f ^ m, 1 - c), in_half(f ^ m, 1 - c), bs.at[m - 1], br.at[m - 1], (f, t ^ 1))
+
+    def in_z():
+        spot = quarter(f ^ deep_m, seat(z % 2))
+        return remote(spot, spot, a_s.at[nf - 1], a_r.at[nf - 1], (f, t ^ 2))
+
+    def in_z_from():
+        spot = quarter(f ^ deep_m, seat(1 - z % 2))
+        return remote(spot, spot, a_s.at[nf - 1], a_r.at[nf - 1], (f, t ^ 2))
+
+    def in_to_z():
+        spot = quarter(f ^ deep_m, seat(1 - z % 2))
+        return remote(spot, spot, bs.at[deep_m - 1], br.at[deep_m - 1], (f, t ^ 1))
 
     masks = by_weight(nf)
+    deep_m = masks[-1]
     zorder = by_weight(nz, True)
     left = {m: 2 for m in masks}
     rings = {(m, s): over_z(m, s) for m in masks for s in range(strips)}
@@ -218,11 +249,20 @@
 
     tile = min(ff, 256)
 
-    def square_grad(m):
-        g = f ^ m
+    def term(m, k):
+        cols = pl.ds(pl.multiple_of((f ^ k) * db, db), db)
+        return contract_last(cot_all[f ^ m, :, cols], dw_all[:, cols])
+
+    def square_start(m):
         if m:
             from_sibling(m).wait_recv()
-        sq[g] = contract_last(cot_all[g], dw_all[...])
+        total = term(m, 0)
+        for k in masks[:-1]:
+            total = total + term(m, k)
+        sq[f ^ m] = total
+
+    def square_end(m):
+        sq[f ^ m] += term(m, masks[-1])
 
     def unit(u):
         m, q, n = u
@@ -248,16 +288,16 @@
 
     def halves(u):
         i = first_slot(u)
-        return remote(part.at[1 - c, :, slots(u)], from_sib.at[:, slots(u)], hs.at[i], hr.at[i], (f, t ^ 1))
+        return remote(part.at[1 - c, :, slots(u)], from_sib.at[:, slots(u)], hs, hr.at[i], (f, t ^ 1))
 
     def spread(u, k):
         i = first_slot(u)
-        return remote(wire.at[k, slots(u)], landed.at[k, slots(u)], ws.at[i], wr.at[i], (f, 2 * (z ^ k) + c))
+        return remote(wire.at[k, slots(u)], landed.at[k, slots(u)], ws, wr.at[i], (f, 2 * (z ^ k) + c))
 
     def spreads(u):
         i = first_slot(u)
         return remote(wire.at[pl.ds(1, nz - 1), slots(u)], landed.at[pl.ds(1, nz - 1), slots(u)],
-                      ws.at[i], wr.at[i], (f, t ^ 2))
+                      ws, wr.at[i], (f, t ^ 2))
 
     def scatter(u):
         halves(u).wait_recv()
@@ -270,19 +310,18 @@
 
     def trade(u):
         i = first_slot(u)
-        return remote(final.at[slots(u)], home(u, f, t), ts.at[i], tr.at[i], (f ^ u[0], t))
+        return remote(final.at[slots(u)], home(u, f, t), ts, tr.at[i], (f ^ u[0], t))
 
     def traded(u):
         i = first_slot(u)
         spot = home(u, f ^ u[0], t)
-        return remote(spot, spot, ts.at[i], tr.at[i], (f ^ u[0], t))
+        return remote(spot, spot, ts, tr.at[i], (f ^ u[0], t))
 
     def finish(u):
         value = part[c, z, slots(u)] + from_sib[z, slots(u)]
-        spreads(u).wait()
+        spreads(u).wait_recv()
         for k in range(1, nz):
             value = value + landed[k, slots(u)].astype(F32)
-        halves(u).wait_send()
         if u[0] == 0:
             got[f, t, pl.ds(u[1], u[2])] = value.astype(BF16)
         else:
@@ -293,18 +332,12 @@
         i = first_slot(u)
         spot = lambda y, cls=0: home(u, f ^ u[0], 2 * y + c)
         return Gather(nz, z, lambda y: (f, 2 * y + c), lambda cls: spot(z), spot,
-                      gs.at[i], lambda cls, k: gr.at[i, k - 1],
-                      ("flat",) if u in late else ("down",))
+                      gs, lambda cls, k: gr.at[i, k - 1],
+                      ("flat",) if u in flats else ("down",))
 
     def over(u, k):
         spot = home(u, f ^ u[0], t ^ (2 * k))
-        i = first_slot(u)
-        return remote(spot, spot, ks.at[i], kr.at[i], (f, t ^ 1))
-
-    def overs(u):
-        i = first_slot(u)
-        spot = landed.at[:, slots(u)]
-        return remote(spot, spot, ks.at[i], kr.at[i], (f, t ^ 1))
+        return remote(spot, spot, ks, kr, (f, t ^ 1))
 
     def announce(u):
         if u[0]:
@@ -341,13 +374,15 @@
     g_cot.push_own()
     own[1].wait()
     g_dw.push_own((0,))
+    for copy in own[2:]:
+        copy.start()
     take_cot(near)
     g_dw.push_own((1,))
     for m, s in near_spots[:2]:
         turn(m, s, ahead_k)
     take(g_dw, inner)
     own[2].wait()
-    g_pa.push_own()
+    g_pa.push_own((0, 1))
     take_cot(far)
     for m, s in near_spots[2:]:
         turn(m, s, ahead_k)
@@ -355,44 +390,39 @@
         turn(m, s, end_k)
     for m, s in far_spots:
         turn(m, s, ahead_k)
-    take(g_dw, outer)
-    for copy in own[3:]:
+    take(g_dw, [p for p in outer if p[0] != masks[-1]])
+    own[3].wait()
+    for m in [0] + singles:
+        square_start(m)
+    take(g_dw, [p for p in outer if p[0] == masks[-1]])
+    for copy in own[4:]:
         copy.wait()
 
-    heads = [(m, q) for j in range(lanes // 2) for q in (j, lanes - 1 - j) for m in masks]
-    inner = [p for p in heads if g_pa.targets(p[1], p[0])]
-    middle = [p for p in heads if p not in inner and single(p)]
-    last = [p for p in heads if p not in inner and not single(p)]
-    first_units = [(0, 0, subs)]
+    first = (0, 0, subs)
     if subs == 1:
-        inner_units, middle_units = [], [(m, 0, 1) for m in singles]
-        last_units = [(m, 0, 1) for m in masks if m not in singles]
+        steps = [[(m, 0, 1)] for m in masks]
     else:
         side = lanes // 2
-        inner_units = [(m, q, side) for m in masks for q in (0, side) if (m, q) in inner]
-        middle_units = [(m, q, side) for m in masks for q in (0, side) if (m, q) in middle]
-        last_units = [(m, q, 1) for m, q in last]
-    early, late = last_units[:len(last_units) // 2], last_units[len(last_units) // 2:]
+        ends = lambda items, j: [(m, q, 1) for m, q in items if q in (j, lanes - 1 - j)]
+        heads = [(m, q) for m in masks for q in range(lanes)]
+        lead = [p for p in heads if g_pa.targets(p[1], p[0])]
+        tail = [p for p in heads if p not in lead and p[0] in singles]
+        deep = [p for p in heads if p not in lead and p[0] not in singles]
+        steps = [ends(lead, j) for j in range(side)] + [ends(deep, j) for j in range(side)]
+        steps += [[(m, q, 1) for m, q in tail if q in ((j, lanes - 1 - j) if m == singles[-1] else (lanes - 1 - j, j))]
+                  for j in range(side - 1, -1, -1)]
+    every = [first] + [u for items in steps for u in items]
+    count = len(steps)
+    flats = [u for items in steps[-2:] for u in items]
     outs = {}
-    every = first_units + inner_units + middle_units + last_units
-    square_grad(0)
-    for u in first_units:
-        unit(u)
-    for m, s in far_spots:
-        turn(m, s, end_k)
-    square_grad(singles[0])
-    for u in first_units:
-        scatter(u)
-    for m in masks[1:]:
-        square_grad(m)
 
     def come(items):
-        for m, cls in items:
-            g_pa.arrive(cls, m)
+        for m, q, n in items:
+            g_pa.arrive(q, m)
 
     def forward(items):
-        for m, cls in items:
-            g_pa.push(cls, m)
+        for m, q, n in items:
+            g_pa.push(q, m)
 
     def settle():
         width = cc // strips
@@ -403,99 +433,120 @@
         g_cot.drain(cot_all.at[pl.ds(0, nf - 1), pl.ds(0, cr), pl.ds(0, cc)])
         g_dw.drain(dw_all.at[:, pl.ds(0, (nf - 1) * db)])
 
-    come(inner)
-    forward(inner[:len(inner) // 2])
-    for u in inner_units:
-        unit(u)
-    for u in first_units:
+    def swap_in(items):
+        for m in items:
+            exchanged(m).wait_recv()
+            in_to(m).start()
+            if m == deep_m:
+                in_z().start()
+
+    def fill(j):
+        for job in jobs.pop(j, []):
+            job()
+
+    def refill(j):
+        if subs == 1:
+            if j == 0:
+                for m in masks:
+                    exchange(m).start()
+            return
+        if j < side:
+            forward(steps[j])
+        elif j < lanes:
+            g_pa.push_own((j,))
+        elif j == lanes:
+            exchange(deep_m).start()
+        else:
+            for m in masks[:-1]:
+                exchange(m).start()
+
+    groups = lambda i: [first] if i < 0 else steps[i]
+
+    def run(i):
+        if subs > 1:
+            come(steps[i])
+        refill(i)
+        for u in steps[i]:
+            unit(u)
+        if 2 <= i < count - 1:
+            for u in groups(i - 3):
+                announce(u)
+        fill(i)
+        for u in steps[i]:
+            scatter(u)
+        if i >= 2 and i == count - 1:
+            for u in groups(i - 3):
+                announce(u)
+        if i == 1:
+            finish(first)
+        for u in steps[i - 1] if i else []:
+            finish(u)
+        if i >= 3:
+            for u in groups(i - 4):
+                pass_on(u, near_k(u))
+
+    near_k = lambda u: [] if u in flats else ahead_k
+    rest_k = lambda u: outs[u].targets(0, 0) if u in flats else end_k
+    jobs = {
+        0: [lambda: square_start(masks[-1]), lambda: square_end(masks[-1])] if subs > 1 else [],
+        1: [settle],
+        2: [lambda: down(0, True)],
+        3: [lambda: up_part(0, True)],
+        4: [lambda: down(masks[-1], False)],
+    }
+
+    square_end(0)
+    unit(first)
+    for m in singles:
+        square_end(m)
+    for m, s in far_spots:
+        turn(m, s, end_k)
+    if subs == 1:
+        for m in masks:
+            if m not in singles:
+                square_start(m)
+                square_end(m)
+        for cls in range(lanes):
+            for m in masks:
+                g_pa.arrive(cls, m)
+                g_pa.push(cls, m)
+    scatter(first)
+    for i in range(count):
+        run(i)
+    for j in sorted(jobs):
+        fill(j)
+    swap_in(masks[-1:])
+    for u in steps[-3]:
+        announce(u)
+    for m in masks if subs == 1 else singles:
+        if not (subs == 1 and m == masks[-1]):
+            down(m, False)
+    for u in steps[-1]:
         finish(u)
-    for u in inner_units:
-        scatter(u)
-    for u in first_units:
+    for u in steps[-4]:
+        pass_on(u, near_k(u))
+    for u in steps[-2]:
         announce(u)
-    settle()
-    down(0, True)
-    up_part(0, True)
-    for u in inner_units:
-        finish(u)
-    forward(inner[len(inner) // 2:])
-    for m in masks:
-        if m not in singles:
-            exchange(m).start()
-    for u in first_units:
-        pass_on(u, ahead_k)
-    take(g_pa, middle)
-    for u in middle_units:
-        unit(u)
-    for u in middle_units:
-        scatter(u)
-    for u in first_units:
-        pass_on(u, end_k)
-    for u in inner_units:
-        announce(u)
-    for m in singles:
-        down(m, False)
-
-    def final_units(items):
-        for u in items:
-            if subs > 1:
-                come([(u[0], u[1])])
-            unit(u)
-        for u in items:
-            scatter(u)
-
-    if subs == 1:
-        take(g_pa, last)
-    final_units(early)
-    for u in middle_units:
-        finish(u)
-    for m in singles:
-        exchange(m).start()
-    final_units(late)
-    for u in inner_units:
-        pass_on(u, ahead_k)
-    for u in middle_units:
-        announce(u)
-    for u in inner_units:
-        pass_on(u, end_k)
-    for u in early:
-        finish(u)
-    for m in masks:
-        if m not in singles:
-            down(m, False)
-    for u in late:
-        finish(u)
     dn_own[...] = jnp.sum(dgrad[...] * dgrad[...], axis=1).reshape(1, ff)
     downs = [remote(dn_own, dn_all.at[f], ds, dr, (f ^ m, t)) for m in range(1, nf)]
     for copy in downs:
         copy.start()
-
-    def swap_in(items):
-        for m in items:
-            exchanged(m).wait_recv()
-            in_to(m).start()
-
-    swap_in([m for m in masks if m not in singles])
-    for u in early:
+    swap_in(masks[:-1])
+    for u in steps[-3]:
+        pass_on(u, near_k(u))
+    for u in steps[-1]:
         announce(u)
-    for u in middle_units:
-        pass_on(u, ahead_k)
-    for u in late:
-        announce(u)
-    swap_in(singles)
-    for m in masks[::-1]:
+    in_z_from().wait_recv()
+    in_to_z().start()
+    for m in masks:
         in_from(m).wait_recv()
         up_part(m, False)
     un_own[...] = jnp.sum(ugrad[...] * ugrad[...], axis=1).reshape(1, db)
     ups = [remote(un_own, un_all.at[t], us, ur, (f, t ^ m)) for m in range(1, nt)]
     for copy in ups:
         copy.start()
-    for u in early:
-        pass_on(u, ahead_k)
-    for u in middle_units + early:
-        pass_on(u, end_k)
-    for u in late:
-        pass_on(u, zorder)
+    for u in [first] + [u for items in steps for u in items]:
+        pass_on(u, rest_k(u))
 
     def up_sums():
         spot = un_all.at[pl.ds(0, nt - 1)]
@@ -514,18 +565,20 @@
     norms_in()
 
     def gathered():
-        for u in every:
-            overs(u).wait_recv()
+        remote(landed, landed, ks, kr, (f, t ^ 1)).wait_recv()
 
     def drain():
-        for u in every:
-            outs[u].drain(landed.at[pl.ds(1, nz - 1), slots(u)])
-            overs(u).wait_send()
-            if u[0]:
-                trade(u).wait_send()
-        spot = inp_all.at[pl.ds(0, nf - 1), pl.ds(0, ih)]
-        remote(spot, spot, a_s, bs, (f, t ^ 1)).wait_send()
-        remote(spot, spot, bs, a_s, (f, t ^ 1)).wait_send()
+        most = landed.at[pl.ds(1, nz - 1)]
+        remote(landed, landed, ks, kr, (f, t ^ 1)).wait_send()
+        remote(most, most, ws, kr, (f, t ^ 2)).wait_send()
+        remote(most, most, gs, kr, (f, t ^ 2)).wait_send()
+        remote(from_sib, from_sib, hs, kr, (f, t ^ 1)).wait_send()
+        traded_all = final.at[pl.ds(subs, (nf - 1) * subs)]
+        remote(traded_all, traded_all, ts, kr, (f ^ 1, t)).wait_send()
+        for m in masks:
+            exchange(m).wait_send()
+            in_from(m).wait_send()
+        in_z().wait_send()
         g_pa.drain(pa_all.at[pl.ds(0, nf - 1)])
         up_sums().wait_send()
         down_sums().wait_send()
@@ -547,10 +600,12 @@
     hbm = pl.BlockSpec(memory_space=pl.ANY)
     V = pltpu.VMEM
     n = nf - 1
-    count = 9 if subs == 4 and nf == 4 else nf
+    cuts = share_rows(rows, nt)
+    count = 1 + n * subs
     sems = [dma((3,)), dma((2, 2, n)), dma((max(subs, 2), n)), dma((n, strips)), dma((n, strips, nz - 1))]
-    sems += [dma((n,)), dma((n,)), dma(()), dma((n,)), dma(()), dma((n,))] + [dma((count,))] * 7
-    sems += [dma((count, nz - 1)), dma((count,)), dma((count,)), dma(()), dma(()), dma(()), dma(()), dma((5,))]
+    sems += [dma((n,)), dma((n,)), dma((nf,)), dma((nf,)), dma((n,)), dma((n,))]
+    sems += [dma(()), dma((count,)), dma(()), dma((count,)), dma(()), dma((count,)), dma(()), dma((count, nz - 1))]
+    sems += [dma(())] * 6 + [dma((7,))]
     return pl.pallas_call(
         functools.partial(fused_kernel, nf, nt, subs, strips),
         out_shape=[
@@ -560,6 +615,7 @@
         in_specs=[hbm] * 5,
         out_specs=[vmem] * 5,
         scratch_shapes=[
+            V((rows // cuts, d * cuts // nt), BF16), V((rows, d), BF16),
             V((nf, rows, d), BF16), V((ff, d), BF16), V((nf, rows, ff), BF16), V((nf, rows, db), BF16),
             V((db, ff), BF16), V((nf, rows, ff), BF16), V((nf, rows, ff), BF16), V((nf, rows, ff), F32),
             V((2, nz, units, pr, pc), F32), V((nz, units, pr, pc), F32),

time: 97.1 us -> 95.1 us (0.979)
  Pallas kernels: 96.3 us -> 94.1 us
    pallas_call x1, Pallas kernels: 93.7 us -> 91.6 us  [fused(): pl.pallas_call(functools.partial(fused_kernel, nf, nt, subs, strips), out...]
where the time goes in v2:
time: 95.1 us; the launch traced here: 94.9 us
  Pallas kernels  94.1 us (99%)
    pallas_call x1, Pallas kernels, fused(): pl.pallas_call(functools.partial(fused_kernel, nf, nt, subs, strips), out...  91.6 us
    pallas_call x1, Pallas kernels, deliver(): pl.pallas_call(deliver_kernel, out_shape=[H(ugrad.shape, F32), H(dgrad.sh...  2.57 us

profile of v2, /device:TPU:0, one launch (start us, length us, event | category | flops | bytes accessed | tf_op | source)
XLA Modules:
  0.0 94.9 jit_solution(4312642787718416135)
XLA Ops:
  0.6 91.6 %shard_map.92 = (f32[512,1024]{1,0:T(8,128)S(1)}, f32[1024,512]{1,0:T(8,128)S(1)}, bf16[4,8,4,48,128]{4,3,2,1,0:T(8,128)(2,1)S(1)}, f32[8,1,512]{2,1,0:T(1,128)S(1)}, f32[4,1,1024]{2,1,0:T(1,128)S(1)}) custom-call(bf16[384,2048]{1,0:T(8,128)(2,1)} %cot.1, bf16[1024,512]{1,0:T(8,128)(2,1)} %dw.1, bf16[384,1024]{1,0:T(8,128)(2,1)} %pa.1, ...), custom_call_target="tpu_custom_call" | custom-call | tf_op jit(solution)/shard_map/pallas_call | solution.py:609
  92.2 2.6 %shard_map.93 = (f32[512,1024]{1,0:T(8,128)}, f32[1024,512]{1,0:T(8,128)}, bf16[384,2048]{1,0:T(8,128)(2,1)}, f32[1,512]{1,0:T(1,128)}, f32[1,1024]{1,0:T(1,128)}) custom-call(f32[512,1024]{1,0:T(8,128)S(1)} %get-tuple-element.15.ugrad, f32[1024,512]{1,0:T(8,128)S(1)} %get-tuple-element.16.dgrad, bf16[4,8,4,48,128]{4,3,2,1,0:T(8,128)(2,1)S(1)} %get-tuple-element.17.got, ...), custom_call_target="tpu_custom_call" | custom-call | tf_op jit(solution)/shard_map/pallas_call | solution.py:662

commit v3 on v2

--- a/solution.py
+++ b/solution.py
@@ -155,9 +155,12 @@
     lanes = max(subs, 2)
     pah = rows // lanes
 
+    def pa_turn(cls, m):
+        return cls * (nf - 1) + m - 1 if subs == 1 else turns[m, cls, 1] - 1
+
     def over_fs(k, source, place, n=2):
         return Gather(nf, f, lambda g: (g, t), source, place, xs.at[k],
-                      lambda cls, m: pa_r.at[cls, m - 1] if k == 2 else xr.at[k, cls, m - 1],
+                      lambda cls, m: pa_r.at[pa_turn(cls, m)] if k == 2 else xr.at[k, cls, m - 1],
                       ("up",) * (n // 2) + ("down",) * (n // 2))
 
     g_cot = over_fs(0, lambda h: cot_own.at[:, pl.ds(h * (cc // 2), cc // 2)], lambda g, h: piece(cot_all.at[g], t, h))
@@ -195,7 +198,12 @@
     def place(m, g):
         return quarter(g, seat(z % 2)) if m == deep_m else in_half(g, c)
 
-    exchange = lambda m: remote(source(m), place(m, f), a_s.at[m - 1], a_r.at[m - 1], (f ^ m, t))
+    def exchange(m, part=None):
+        src, dst = source(m), place(m, f)
+        if part is not None:
+            src, dst = src.at[pl.ds(part * iq, iq)], dst.at[pl.ds(part * iq, iq)]
+        return remote(src, dst, a_s.at[m - 1], a_r.at[m - 1], (f ^ m, t))
+
     exchanged = lambda m: remote(place(m, f ^ m), place(m, f ^ m), a_s.at[m - 1], a_r.at[m - 1], (f ^ m, t))
     in_to = lambda m: remote(place(m, f ^ m), place(m, f ^ m), bs.at[m - 1], br.at[m - 1], (f, t ^ 1))
 
@@ -283,7 +291,7 @@
         halves(u).start()
 
     wide = height // 2 == pr
-    first_slot = lambda u: every.index(u)
+    first_slot = lambda u: turns[u]
     slots = lambda u: pl.ds(u[0] * subs + u[1], u[2])
 
     def halves(u):
@@ -294,16 +302,18 @@
         i = first_slot(u)
         return remote(wire.at[k, slots(u)], landed.at[k, slots(u)], ws, wr.at[i], (f, 2 * (z ^ k) + c))
 
-    def spreads(u):
-        i = first_slot(u)
-        return remote(wire.at[pl.ds(1, nz - 1), slots(u)], landed.at[pl.ds(1, nz - 1), slots(u)],
-                      ws, wr.at[i], (f, t ^ 2))
-
-    def scatter(u):
-        halves(u).wait_recv()
-        for k in range(nz - 1, 0, -1):
-            wire[k, slots(u)] = (part[c, z ^ k, slots(u)] + from_sib[z ^ k, slots(u)]).astype(BF16)
-            spread(u, k).start()
+    def scatter(items):
+        arrived(from_sib.at[:, group_slots(items)], hr.at[turns[items[0]]])
+        for u in items:
+            for k in range(nz - 1, 0, -1):
+                wire[k, slots(u)] = (part[c, z ^ k, slots(u)] + from_sib[z ^ k, slots(u)]).astype(BF16)
+                spread(u, k).start()
+
+    def group_slots(items):
+        return pl.ds(0, sum(u[2] for u in items))
+
+    def arrived(spot, sem):
+        remote(spot, spot, hs, sem, (f, t ^ 1)).wait_recv()
 
     def home(u, g, k):
         return got.at[g, k, pl.ds(u[1], u[2])]
@@ -312,45 +322,45 @@
         i = first_slot(u)
         return remote(final.at[slots(u)], home(u, f, t), ts, tr.at[i], (f ^ u[0], t))
 
-    def traded(u):
-        i = first_slot(u)
-        spot = home(u, f ^ u[0], t)
-        return remote(spot, spot, ts, tr.at[i], (f ^ u[0], t))
-
-    def finish(u):
-        value = part[c, z, slots(u)] + from_sib[z, slots(u)]
-        spreads(u).wait_recv()
-        for k in range(1, nz):
-            value = value + landed[k, slots(u)].astype(F32)
-        if u[0] == 0:
-            got[f, t, pl.ds(u[1], u[2])] = value.astype(BF16)
-        else:
-            final[slots(u)] = value.astype(BF16)
-            trade(u).start()
+    def finish(items):
+        arrived(landed.at[pl.ds(1, nz - 1), group_slots(items)], wr.at[turns[items[0]]])
+        for u in items:
+            value = part[c, z, slots(u)] + from_sib[z, slots(u)]
+            for k in range(1, nz):
+                value = value + landed[k, slots(u)].astype(F32)
+            if u[0] == 0:
+                got[f, t, pl.ds(u[1], u[2])] = value.astype(BF16)
+            else:
+                final[slots(u)] = value.astype(BF16)
+                trade(u).start()
 
     def ring_of(u):
         i = first_slot(u)
         spot = lambda y, cls=0: home(u, f ^ u[0], 2 * y + c)
         return Gather(nz, z, lambda y: (f, 2 * y + c), lambda cls: spot(z), spot,
-                      gs, lambda cls, k: gr.at[i, k - 1],
+                      gs, lambda cls, k: gr.at[i, ahead_k.index(k) if k in ahead_k and u not in flats else len(ahead_k)],
                       ("flat",) if u in flats else ("down",))
 
     def over(u, k):
         spot = home(u, f ^ u[0], t ^ (2 * k))
         return remote(spot, spot, ks, kr, (f, t ^ 1))
 
-    def announce(u):
-        if u[0]:
-            traded(u).wait_recv()
-        outs[u] = ring_of(u)
-        outs[u].push(0, 0)
-        over(u, 0).start()
-
-    def pass_on(u, steps):
-        for k in steps:
-            outs[u].arrive(0, k)
-            outs[u].push(0, k)
-            over(u, k).start()
+    def announce(items):
+        if items[0][0]:
+            arrived(final.at[group_slots(items)], tr.at[turns[items[0]]])
+        for u in items:
+            outs[u] = ring_of(u)
+            outs[u].push(0, 0)
+            over(u, 0).start()
+
+    def pass_on(items, steps_k, which):
+        if not steps_k:
+            return
+        arrived(landed.at[pl.ds(0, len(steps_k)), group_slots(items)], gr.at[turns[items[0]], which])
+        for k in steps_k:
+            for u in items:
+                outs[u].push(0, k)
+                over(u, k).start()
 
     def down(m, first):
         g = f ^ m
@@ -381,6 +391,23 @@
     for m, s in near_spots[:2]:
         turn(m, s, ahead_k)
     take(g_dw, inner)
+    first = (0, 0, subs)
+    if subs == 1:
+        steps = [[(m, 0, 1)] for m in masks]
+    else:
+        side = lanes // 2
+        ends = lambda items, j: [(m, q, 1) for m, q in items if q in (j, lanes - 1 - j)]
+        heads = [(m, q) for m in masks for q in range(lanes)]
+        lead = [p for p in heads if g_pa.targets(p[1], p[0])]
+        tail = [p for p in heads if p not in lead and p[0] in singles]
+        deep = [p for p in heads if p not in lead and p[0] not in singles]
+        steps = [ends(lead, j) for j in range(side)] + [ends(deep, j) for j in range(side)]
+        steps += [[(m, q, 1) for m, q in tail if q in ((j, lanes - 1 - j) if m == singles[-1] else (lanes - 1 - j, j))]
+                  for j in range(side - 1, -1, -1)]
+    count = len(steps)
+    turns = {u: i + 1 for i, items in enumerate(steps) for u in items}
+    turns[first] = 0
+    flats = [u for items in steps[-3:] for u in items]
     own[2].wait()
     g_pa.push_own((0, 1))
     take_cot(far)
@@ -398,27 +425,10 @@
     for copy in own[4:]:
         copy.wait()
 
-    first = (0, 0, subs)
-    if subs == 1:
-        steps = [[(m, 0, 1)] for m in masks]
-    else:
-        side = lanes // 2
-        ends = lambda items, j: [(m, q, 1) for m, q in items if q in (j, lanes - 1 - j)]
-        heads = [(m, q) for m in masks for q in range(lanes)]
-        lead = [p for p in heads if g_pa.targets(p[1], p[0])]
-        tail = [p for p in heads if p not in lead and p[0] in singles]
-        deep = [p for p in heads if p not in lead and p[0] not in singles]
-        steps = [ends(lead, j) for j in range(side)] + [ends(deep, j) for j in range(side)]
-        steps += [[(m, q, 1) for m, q in tail if q in ((j, lanes - 1 - j) if m == singles[-1] else (lanes - 1 - j, j))]
-                  for j in range(side - 1, -1, -1)]
-    every = [first] + [u for items in steps for u in items]
-    count = len(steps)
-    flats = [u for items in steps[-2:] for u in items]
     outs = {}
 
     def come(items):
-        for m, q, n in items:
-            g_pa.arrive(q, m)
+        arrived(pa_all.at[0, pl.ds(0, len(items) * pah)], pa_r.at[turns[items[0]] - 1])
 
     def forward(items):
         for m, q, n in items:
@@ -458,9 +468,18 @@
             exchange(deep_m).start()
         else:
             for m in masks[:-1]:
-                exchange(m).start()
+                exchange(m, 0).start()
 
     groups = lambda i: [first] if i < 0 else steps[i]
+    near_k = lambda items: [] if items[0] in flats else ahead_k
+    rest_k = lambda items: outs[items[0]].targets(0, 0) if items[0] in flats else end_k
+
+    def near_pass(items):
+        for j, k in enumerate(near_k(items)):
+            pass_on(items, [k], j)
+
+    def rest_pass(items):
+        pass_on(items, rest_k(items), len(ahead_k))
 
     def run(i):
         if subs > 1:
@@ -468,25 +487,17 @@
         refill(i)
         for u in steps[i]:
             unit(u)
-        if 2 <= i < count - 1:
-            for u in groups(i - 3):
-                announce(u)
+        if 2 <= i:
+            announce(groups(i - 3))
         fill(i)
-        for u in steps[i]:
-            scatter(u)
-        if i >= 2 and i == count - 1:
-            for u in groups(i - 3):
-                announce(u)
+        scatter(steps[i])
         if i == 1:
-            finish(first)
-        for u in steps[i - 1] if i else []:
-            finish(u)
-        if i >= 3:
-            for u in groups(i - 4):
-                pass_on(u, near_k(u))
-
-    near_k = lambda u: [] if u in flats else ahead_k
-    rest_k = lambda u: outs[u].targets(0, 0) if u in flats else end_k
+            finish([first])
+        if i:
+            finish(steps[i - 1])
+        if i >= 3 and (i < count - 1 or subs == 1):
+            near_pass(groups(i - 4))
+
     jobs = {
         0: [lambda: square_start(masks[-1]), lambda: square_end(masks[-1])] if subs > 1 else [],
         1: [settle],
@@ -510,34 +521,33 @@
             for m in masks:
                 g_pa.arrive(cls, m)
                 g_pa.push(cls, m)
-    scatter(first)
+    scatter([first])
     for i in range(count):
         run(i)
     for j in sorted(jobs):
         fill(j)
-    swap_in(masks[-1:])
-    for u in steps[-3]:
-        announce(u)
+    if subs > 1:
+        for m in masks[:-1]:
+            exchange(m, 1).start()
+    if subs > 1:
+        near_pass(steps[-5])
     for m in masks if subs == 1 else singles:
         if not (subs == 1 and m == masks[-1]):
             down(m, False)
-    for u in steps[-1]:
-        finish(u)
-    for u in steps[-4]:
-        pass_on(u, near_k(u))
-    for u in steps[-2]:
-        announce(u)
+    swap_in(masks[-1:])
+    announce(steps[-3])
+    announce(steps[-2])
+    finish(steps[-1])
+    near_pass(steps[-4])
     dn_own[...] = jnp.sum(dgrad[...] * dgrad[...], axis=1).reshape(1, ff)
     downs = [remote(dn_own, dn_all.at[f], ds, dr, (f ^ m, t)) for m in range(1, nf)]
     for copy in downs:
         copy.start()
     swap_in(masks[:-1])
-    for u in steps[-3]:
-        pass_on(u, near_k(u))
-    for u in steps[-1]:
-        announce(u)
+    announce(steps[-1])
     in_z_from().wait_recv()
     in_to_z().start()
+    near_pass(steps[-3])
     for m in masks:
         in_from(m).wait_recv()
         up_part(m, False)
@@ -545,8 +555,8 @@
     ups = [remote(un_own, un_all.at[t], us, ur, (f, t ^ m)) for m in range(1, nt)]
     for copy in ups:
         copy.start()
-    for u in [first] + [u for items in steps for u in items]:
-        pass_on(u, rest_k(u))
+    for items in [[first]] + steps:
+        rest_pass(items)
 
     def up_sums():
         spot = un_all.at[pl.ds(0, nt - 1)]
@@ -601,10 +611,10 @@
     V = pltpu.VMEM
     n = nf - 1
     cuts = share_rows(rows, nt)
-    count = 1 + n * subs
-    sems = [dma((3,)), dma((2, 2, n)), dma((max(subs, 2), n)), dma((n, strips)), dma((n, strips, nz - 1))]
+    count = 7 if subs > 1 else 1 + n
+    sems = [dma((3,)), dma((2, 2, n)), dma((2 * n,)), dma((n, strips)), dma((n, strips, nz - 1))]
     sems += [dma((n,)), dma((n,)), dma((nf,)), dma((nf,)), dma((n,)), dma((n,))]
-    sems += [dma(()), dma((count,)), dma(()), dma((count,)), dma(()), dma((count,)), dma(()), dma((count, nz - 1))]
+    sems += [dma(()), dma((count,)), dma(()), dma((count,)), dma(()), dma((count,)), dma(()), dma((count, nz // 2))]
     sems += [dma(())] * 6 + [dma((7,))]
     return pl.pallas_call(
         functools.partial(fused_kernel, nf, nt, subs, strips),
@@ -630,7 +640,7 @@
     nf, nt, subs, pr, pc = got.shape
     rows, d = whole.shape
     half, db = rows // subs, d // nf
-    copies = [pltpu.make_async_copy(ugrad, ug_out, sem.at[0]), pltpu.make_async_copy(dgrad, dg_out, sem.at[1])]
+    copies = [pltpu.make_async_copy(ugrad, ug_out, sem.at[3]), pltpu.make_async_copy(dgrad, dg_out, sem.at[4])]
     for copy in copies:
         copy.start()
     wide = half // 2 == pr
@@ -646,8 +656,8 @@
         dn = dn + dn_all[k]
     un_sum[...] = un
     dn_sum[...] = dn
-    last = [pltpu.make_async_copy(whole, out, sem.at[2]), pltpu.make_async_copy(un_sum, un_out, sem.at[3]),
-            pltpu.make_async_copy(dn_sum, dn_out, sem.at[4])]
+    last = [pltpu.make_async_copy(whole, out, sem.at[0]), pltpu.make_async_copy(un_sum, un_out, sem.at[1]),
+            pltpu.make_async_copy(dn_sum, dn_out, sem.at[2])]
     for copy in last:
         copy.start()
     for copy in copies + last:

time: 95.1 us -> 93.5 us (0.983)
  Pallas kernels: 94.1 us -> 92.6 us
    pallas_call x1, Pallas kernels: 91.6 us -> 90 us  [fused(): pl.pallas_call(functools.partial(fused_kernel, nf, nt, subs, strips), out...]
where the time goes in v3:
time: 93.5 us; the launch traced here: 93.4 us
  Pallas kernels  92.6 us (99%)
    pallas_call x1, Pallas kernels, fused(): pl.pallas_call(functools.partial(fused_kernel, nf, nt, subs, strips), out...  90 us
    pallas_call x1, Pallas kernels, deliver(): pl.pallas_call(deliver_kernel, out_shape=[H(ugrad.shape, F32), H(dgrad.sh...  2.57 us

profile of v3, /device:TPU:0, one launch (start us, length us, event | category | flops | bytes accessed | tf_op | source)
XLA Modules:
  0.0 93.4 jit_solution(10710395447836570451)
XLA Ops:
  0.6 90.0 %shard_map.92 = (f32[512,1024]{1,0:T(8,128)S(1)}, f32[1024,512]{1,0:T(8,128)S(1)}, bf16[4,8,4,48,128]{4,3,2,1,0:T(8,128)(2,1)S(1)}, f32[8,1,512]{2,1,0:T(1,128)S(1)}, f32[4,1,1024]{2,1,0:T(1,128)S(1)}) custom-call(bf16[384,2048]{1,0:T(8,128)(2,1)} %cot.1, bf16[1024,512]{1,0:T(8,128)(2,1)} %dw.1, bf16[384,1024]{1,0:T(8,128)(2,1)} %pa.1, ...), custom_call_target="tpu_custom_call" | custom-call | tf_op jit(solution)/shard_map/pallas_call | solution.py:619
  90.7 2.6 %shard_map.93 = (f32[512,1024]{1,0:T(8,128)}, f32[1024,512]{1,0:T(8,128)}, bf16[384,2048]{1,0:T(8,128)(2,1)}, f32[1,512]{1,0:T(1,128)}, f32[1,1024]{1,0:T(1,128)}) custom-call(f32[512,1024]{1,0:T(8,128)S(1)} %get-tuple-element.15.ugrad, f32[1024,512]{1,0:T(8,128)S(1)} %get-tuple-element.16.dgrad, bf16[4,8,4,48,128]{4,3,2,1,0:T(8,128)(2,1)S(1)} %get-tuple-element.17.got, ...), custom_call_target="tpu_custom_call" | custom-call | tf_op jit(solution)/shard_map/pallas_call | solution.py:672

commit v4 on v3

--- a/solution.py
+++ b/solution.py
@@ -362,14 +362,16 @@
                 outs[u].push(0, k)
                 over(u, k).start()
 
-    def down(m, first):
-        g = f ^ m
-        value = contract_first(sqr[g], cot_all[g, :, own_cols])
+    def stacked(items, read):
+        values = [read(f ^ m) for m in items]
+        return values[0] if len(values) == 1 else jnp.concatenate(values, axis=0)
+
+    def down(items, first=False):
+        value = contract_first(stacked(items, lambda g: sqr[g]), stacked(items, lambda g: cot_all[g, :, own_cols]))
         dgrad[...] = value if first else dgrad[...] + value
 
-    def up_part(m, first):
-        g = f ^ m
-        value = contract_first(inp_all[g], pre[g])
+    def up_part(items, first=False):
+        value = contract_first(stacked(items, lambda g: inp_all[g]), stacked(items, lambda g: pre[g]))
         ugrad[...] = value if first else ugrad[...] + value
 
     single = lambda p: p[0] in singles
@@ -501,9 +503,9 @@
     jobs = {
         0: [lambda: square_start(masks[-1]), lambda: square_end(masks[-1])] if subs > 1 else [],
         1: [settle],
-        2: [lambda: down(0, True)],
-        3: [lambda: up_part(0, True)],
-        4: [lambda: down(masks[-1], False)],
+        2: [lambda: down([0], True)],
+        3: [lambda: up_part([0], True)],
+        4: [lambda: down([masks[-1]])],
     }
 
     square_end(0)
@@ -531,12 +533,12 @@
             exchange(m, 1).start()
     if subs > 1:
         near_pass(steps[-5])
-    for m in masks if subs == 1 else singles:
-        if not (subs == 1 and m == masks[-1]):
-            down(m, False)
     swap_in(masks[-1:])
     announce(steps[-3])
     announce(steps[-2])
+    rest = masks[:-1] if subs == 1 else singles
+    for j in range(0, len(rest), 2):
+        down(rest[j:j + 2])
     finish(steps[-1])
     near_pass(steps[-4])
     dn_own[...] = jnp.sum(dgrad[...] * dgrad[...], axis=1).reshape(1, ff)
@@ -548,9 +550,10 @@
     in_z_from().wait_recv()
     in_to_z().start()
     near_pass(steps[-3])
-    for m in masks:
-        in_from(m).wait_recv()
-        up_part(m, False)
+    for j in range(0, len(masks), 2):
+        for m in masks[j:j + 2]:
+            in_from(m).wait_recv()
+        up_part(masks[j:j + 2])
     un_own[...] = jnp.sum(ugrad[...] * ugrad[...], axis=1).reshape(1, db)
     ups = [remote(un_own, un_all.at[t], us, ur, (f, t ^ m)) for m in range(1, nt)]
     for copy in ups:

time: 93.5 us -> 93.3 us (level)
  no operation moved by 1% of the time
where the time goes in v4:
time: 93.3 us; the launch traced here: 93.2 us
  Pallas kernels  92.4 us (99%)
    pallas_call x1, Pallas kernels, fused(): pl.pallas_call(functools.partial(fused_kernel, nf, nt, subs, strips), out...  89.8 us
    pallas_call x1, Pallas kernels, deliver(): pl.pallas_call(deliver_kernel, out_shape=[H(ugrad.shape, F32), H(dgrad.sh...  2.57 us

profile of v4, /device:TPU:0, one launch (start us, length us, event | category | flops | bytes accessed | tf_op | source)
XLA Modules:
  0.0 93.2 jit_solution(8028599229402009507)
XLA Ops:
  0.6 89.8 %shard_map.92 = (f32[512,1024]{1,0:T(8,128)S(1)}, f32[1024,512]{1,0:T(8,128)S(1)}, bf16[4,8,4,48,128]{4,3,2,1,0:T(8,128)(2,1)S(1)}, f32[8,1,512]{2,1,0:T(1,128)S(1)}, f32[4,1,1024]{2,1,0:T(1,128)S(1)}) custom-call(bf16[384,2048]{1,0:T(8,128)(2,1)} %cot.1, bf16[1024,512]{1,0:T(8,128)(2,1)} %dw.1, bf16[384,1024]{1,0:T(8,128)(2,1)} %pa.1, ...), custom_call_target="tpu_custom_call" | custom-call | tf_op jit(solution)/shard_map/pallas_call | solution.py:622
  90.4 2.6 %shard_map.93 = (f32[512,1024]{1,0:T(8,128)}, f32[1024,512]{1,0:T(8,128)}, bf16[384,2048]{1,0:T(8,128)(2,1)}, f32[1,512]{1,0:T(1,128)}, f32[1,1024]{1,0:T(1,128)}) custom-call(f32[512,1024]{1,0:T(8,128)S(1)} %get-tuple-element.15.ugrad, f32[1024,512]{1,0:T(8,128)S(1)} %get-tuple-element.16.dgrad, bf16[4,8,4,48,128]{4,3,2,1,0:T(8,128)(2,1)S(1)} %get-tuple-element.17.got, ...), custom_call_target="tpu_custom_call" | custom-call | tf_op jit(solution)/shard_map/pallas_call | solution.py:675
